TPU v7x, 32 devices: a whole 2x2x4 slice. The times are simulated.
32 devices in a mesh: grp: 2 (over y), fs: 4 (over z), tp: 4 (over x, core).
Axes of the slice: x: 2, y: 2, z: 4, core: 2. Of those that a mesh axis runs over, the one named last changes fastest.
Arguments:
- tokens: bfloat16 [8, 1024, 2048], P(('grp', 'fs'), None, 'tp'), parts along dimension 0, may hold values from -6 to 6
- mix_gain: float32 [2048], replicated, may hold values from 0.1 to 1.9
- in_matrix: float32 [2048, 1024], P('fs', 'tp'), may hold values from -0.125 to 0.125
- in_scale: float32 [1, 1024], P(None, 'tp'), may hold values from 0.5 to 2
- pool_mix: bfloat16 [8, 128, 128], P('tp'), may hold values from -0.5 to 0.5
- pool_scale: float32 [1, 1024], P(None, 'tp'), may hold values from 0.1 to 1.9
- out_matrix: float32 [1024, 2048], P('tp', 'fs'), may hold values from -0.25 to 0.25
- out_scale: float32 [1, 2048], P(None, 'fs'), may hold values from 0.5 to 2
- ffn_gain: float32 [2048], replicated, may hold values from 0.1 to 1.9
- gate_matrix: float32 [2048, 5632], P('fs', 'tp'), may hold values from -0.125 to 0.125
- gate_scale: float32 [1, 5632], P(None, 'tp'), may hold values from 0.5 to 2
- up_matrix: float32 [2048, 5632], P('fs', 'tp'), may hold values from -0.125 to 0.125
- up_scale: float32 [1, 5632], P(None, 'tp'), may hold values from 0.5 to 2
- gate_taps: float32 [3, 5632], P(None, 'tp'), may hold values from -4 to 4
- up_taps: float32 [3, 5632], P(None, 'tp'), may hold values from -4 to 4
- down_matrix: float32 [5632, 2048], P('tp', 'fs'), may hold values from -0.109375 to 0.109375
- down_scale: float32 [1, 2048], P(None, 'fs'), may hold values from 0.5 to 2
Outputs:
- layer_out: bfloat16 [8, 1024, 2048], P(('grp', 'fs'), None, 'tp'), parts along dimension 0
There are 2 independent parts, one for each index of `grp`. A program takes and returns all parts, laid end to end along the dimension named above; an argument that names none is the same for every part. Nothing has to cross between parts.
All inputs are finite; a program needn't handle non-finite values.
Results may differ from a plain program's by a relative error of at most 0.025.
Values may be sent and summed in bfloat16 or wider, within the bound.
A program may use at most 128 MiB of HBM per device.

v0:
```python
import jax
import jax.numpy as jnp
from jax import lax
from jax.sharding import PartitionSpec as P

BLOCKS = 8


eps = 1e-06
widest_span = 16


def norm_rows(tok_rows, norm_gain):
    values = tok_rows.astype(jnp.float32)
    scaled = values * lax.rsqrt(jnp.mean(values * values, axis=-1, keepdims=True) + eps)
    return (scaled * norm_gain).astype(jnp.bfloat16)


def span_widths(block_ids):
    return jnp.left_shift(jnp.ones_like(block_ids), 1 + 4 * block_ids // BLOCKS)


def trailing_gap(projected, windows):
    values = projected.astype(jnp.float32)
    length = values.shape[0]
    running = values
    for offset in range(1, widest_span):
        shifted = jnp.pad(values[: length - offset], ((offset, 0), (0, 0)))
        running = running + jnp.where(windows[None, :] > offset, shifted, jnp.zeros_like(shifted))
    positions = jnp.arange(length, dtype=jnp.int32)[:, None]
    counts = jnp.minimum(positions + 1, windows[None, :]).astype(jnp.float32)
    return (running / counts - values).astype(jnp.bfloat16)


def causal_taps(linear, tap_table):
    values = linear.astype(jnp.float32)
    length = values.shape[0]
    back_one = jnp.pad(values[: length - 1], ((1, 0), (0, 0)))
    back_two = jnp.pad(values[: length - 2], ((2, 0), (0, 0)))
    return tap_table[2] * values + tap_table[1] * back_one + tap_table[0] * back_two


def fold_rows(operand, portion):
    return jnp.dot(operand, portion, preferred_element_type=jnp.float32)


def shards(
    tokens,
    mix_gain,
    in_matrix,
    in_scale,
    pool_mix,
    pool_scale,
    out_matrix,
    out_scale,
    ffn_gain,
    gate_matrix,
    gate_scale,
    up_matrix,
    up_scale,
    gate_taps,
    up_taps,
    down_matrix,
    down_scale,
):
    length = tokens.shape[1]
    own_width = tokens.shape[2]
    local_rows = tokens.reshape(length, own_width)
    gathered = lax.all_gather(local_rows, "tp", axis=1, tiled=True)
    normed = norm_rows(gathered, mix_gain)
    width_in = in_matrix.shape[1]
    in_total = fold_rows(
        normed, lax.all_gather(in_matrix.astype(jnp.bfloat16), "fs", axis=0, tiled=True)
    )
    projected = (in_total * in_scale).astype(jnp.bfloat16)
    local_blocks = pool_mix.shape[0]
    block_width = pool_mix.shape[1]
    block_ids = lax.axis_index("tp") * local_blocks + jnp.arange(local_blocks, dtype=jnp.int32)
    windows = jnp.repeat(span_widths(block_ids), block_width)
    spread = trailing_gap(projected, windows)
    block_mixed = jnp.einsum(
        "lbc,bce->lbe",
        spread.reshape(length, local_blocks, block_width),
        pool_mix,
        preferred_element_type=jnp.float32,
    ).reshape(length, width_in)
    pooled = (block_mixed * pool_scale).astype(jnp.bfloat16)
    out_cols = lax.all_gather(out_scale, "fs", axis=1, tiled=True)
    tp_index = lax.axis_index("tp")
    groups = lax.axis_size("tp")
    pooled_all = lax.all_gather(pooled, "tp", axis=1, tiled=True)
    row_block = lax.all_gather(out_matrix.astype(jnp.bfloat16), "fs", axis=1, tiled=True)
    own_matrix = lax.all_to_all(row_block, "tp", split_axis=1, concat_axis=0, tiled=True)
    own_scales = lax.dynamic_slice_in_dim(out_cols, tp_index * own_width, own_width, 1)
    grouped_rows = pooled_all.reshape(length, groups, width_in)
    grouped_matrix = own_matrix.reshape(groups, width_in, own_width)
    pieces = (
        jnp.einsum("lgc,gcd->gld", grouped_rows, grouped_matrix, preferred_element_type=jnp.float32)
        * own_scales[None]
    )
    rounded = lax.optimization_barrier(pieces.astype(jnp.bfloat16))
    mixing = jnp.sum(rounded.astype(jnp.float32), axis=0)
    residual = (local_rows.astype(jnp.float32) + mixing).astype(jnp.bfloat16)
    gathered_ffn = lax.all_gather(residual, "tp", axis=1, tiled=True)
    normed_ffn = norm_rows(gathered_ffn, ffn_gain)
    gate_cast = gate_matrix.astype(jnp.bfloat16)
    up_cast = up_matrix.astype(jnp.bfloat16)
    gate_full, up_full = (
        lax.all_gather(gate_cast, "fs", axis=0, tiled=True),
        lax.all_gather(up_cast, "fs", axis=0, tiled=True),
    )
    gate_total = jnp.dot(normed_ffn, gate_full, preferred_element_type=jnp.float32)
    up_total = jnp.dot(normed_ffn, up_full, preferred_element_type=jnp.float32)
    gate_lin = (gate_total * gate_scale).astype(jnp.bfloat16)
    up_lin = (up_total * up_scale).astype(jnp.bfloat16)
    hidden = (jax.nn.silu(causal_taps(gate_lin, gate_taps)) * causal_taps(up_lin, up_taps)).astype(
        jnp.bfloat16
    )
    down_cols = lax.all_gather(down_scale, "fs", axis=1, tiled=True)
    partial_ffn = (
        jnp.dot(
            hidden,
            lax.all_gather(down_matrix.astype(jnp.bfloat16), "fs", axis=1, tiled=True),
            preferred_element_type=jnp.float32,
        )
        * down_cols
    )
    feed_out = lax.psum_scatter(
        partial_ffn.astype(jnp.bfloat16), "tp", scatter_dimension=1, tiled=True
    ).astype(jnp.float32)
    result = (residual.astype(jnp.float32) + feed_out).astype(jnp.bfloat16)
    return result.reshape(1, length, result.shape[1])


def solution(mesh):
    return jax.shard_map(
        shards,
        mesh=mesh,
        in_specs=(
            P(("grp", "fs"), None, "tp"),
            P(),
            P("fs", "tp"),
            P(None, "tp"),
            P("tp", None, None),
            P(None, "tp"),
            P("tp", "fs"),
            P(None, "fs"),
            P(),
            P("fs", "tp"),
            P(None, "tp"),
            P("fs", "tp"),
            P(None, "tp"),
            P(None, "tp"),
            P(None, "tp"),
            P("tp", "fs"),
            P(None, "fs"),
        ),
        out_specs=P(("grp", "fs"), None, "tp"),
        check_vma=False,
    )
```

profile of v0, /device:TPU:0, one launch (start us, length us, event | category | flops | bytes accessed | tf_op | source)
XLA Modules:
  0.0 573.4 jit_solution(17679194408588764987)
XLA Ops:
  11.3 34.8 %all-gather.24.cloned.1.call-done = bf16[1,1024,2048]{2,1,0:T(8,128)(2,1)} async-done(((bf16[1,1024,512]{2,1,0:T(8,128)(2,1)}), bf16[1,1024,2048]{2,1,0:T(8,128)(2,1)}) %all-gather.24.cloned.1.call-update) | async-done | bytes 4194320 | tf_op jit(solution)/shard_map/all_gather | solution.py:69
  46.1 3.1 fusion.3
  49.2 26.5 %all-gather.10.cloned.1.call-done = bf16[2048,256]{1,0:T(8,128)(2,1)} async-done(((bf16[512,256]{1,0:T(8,128)(2,1)}), bf16[2048,256]{1,0:T(8,128)(2,1)}) %all-gather.10.cloned.1.call-update) | async-done | bytes 1048592 | tf_op jit(solution)/shard_map/all_gather | solution.py:73
  75.7 3.8 fusion.20
  80.1 3.2 fusion.28
  84.3 20.3 %all-gather.14.cloned.1.call-done = bf16[256,2048]{0,1:T(8,128)(2,1)} async-done(((bf16[256,512]{0,1:T(8,128)(2,1)}), bf16[256,2048]{0,1:T(8,128)(2,1)}) %all-gather.14.cloned.1.call-update) | async-done | bytes 1048592 | tf_op jit(solution)/shard_map/all_gather | solution.py:92
  104.7 2.3 copy.23
  106.9 3.5 all-to-all-start
  110.5 11.9 %all_gather.34 = f32[1,2048]{1,0:T(1,128)S(1)} all-gather(f32[1,512]{1,0:T(1,128)S(1)} %copy-done.10), channel_id=1, replica_groups=mesh['grp'=2,'fs'=4,'tp'=4] {'fs'}, dimensions={1}, use_global_device_ids=true | all-gather | bytes 10240 | tf_op jit(solution)/shard_map/all_gather | solution.py:88
  122.5 12.5 %all-to-all-done = bf16[256,4,512]{2,0,1:T(8,128)(2,1)S(1)} async-done(((bf16[256,4,512]{2,0,1:T(8,128)(2,1)}), bf16[256,4,512]{2,0,1:T(8,128)(2,1)S(1)}, u32[]{:S(2)}, u32[]{:S(2)}) %all-to-all-start) | async-done | bytes 1048608 | tf_op jit(solution)/shard_map/all_to_all | solution.py:93
  135.0 2.7 all-gather.12.cloned.1.call-done
  137.6 3.0 multiply_convert_fusion.1
  144.2 3.3 convert_element_type.136
  149.0 12.1 %all_gather.39 = f32[1,2048]{1,0:T(1,128)S(1)} all-gather(f32[1,512]{1,0:T(1,128)S(1)} %copy-done.11), channel_id=1, replica_groups=mesh['grp'=2,'fs'=4,'tp'=4] {'fs'}, dimensions={1}, use_global_device_ids=true | all-gather | bytes 10240 | tf_op jit(solution)/shard_map/all_gather | solution.py:119
  161.2 14.5 %all-gather.16.cloned.1.call-done = bf16[1024,2048]{1,0:T(8,128)(2,1)} async-done(((bf16[1024,512]{1,0:T(8,128)(2,1)}), bf16[1024,2048]{1,0:T(8,128)(2,1)}) %all-gather.16.cloned.1.call-update) | async-done | bytes 4194320 | tf_op jit(solution)/shard_map/all_gather | solution.py:104
  175.7 3.1 fusion
  178.8 105.1 %all-gather.18.cloned.1.call-done = bf16[2048,1408]{1,0:T(8,128)(2,1)} async-done(((bf16[512,1408]{1,0:T(8,128)(2,1)}), bf16[2048,1408]{1,0:T(8,128)(2,1)}) %all-gather.18.cloned.1.call-update) | async-done | bytes 5767184 | tf_op jit(solution)/shard_map/all_gather | solution.py:109
  283.9 11.9 %fusion.11 = f32[1024,1408]{1,0:T(8,128)} fusion(bf16[2048,1408]{1,0:T(8,128)(2,1)} %all-gather.18.cloned.1.call-done, f32[1408]{0:T(1024)S(1)} %reduce.1, bf16[1024,2048]{1,0:T(8,128)(2,1)} %all-gather.16.cloned.1.call-done, f32[2048]{0:T(1024)S(1)} %copy-done.14, f32[1024]{0:T(1024)S(1)} %add_rsqrt_fusion), kind=kOutput, calls=%fused_computation.20 | convolution fusion | flops 5918294016 | bytes 15746560 | tf_op jit(solution)/shard_map/dot_general | solution.py:112
  295.8 94.7 %all-gather.20.cloned.1.call-done = bf16[2048,1408]{1,0:T(8,128)(2,1)} async-done(((bf16[512,1408]{1,0:T(8,128)(2,1)}), bf16[2048,1408]{1,0:T(8,128)(2,1)}) %all-gather.20.cloned.1.call-update) | async-done | bytes 5767184 | tf_op jit(solution)/shard_map/all_gather | solution.py:110
  390.4 12.0 %fusion.12 = f32[1024,1408]{1,0:T(8,128)} fusion(bf16[2048,1408]{1,0:T(8,128)(2,1)} %all-gather.20.cloned.1.call-done, f32[1408]{0:T(1024)S(1)} %reduce.5, bf16[1024,2048]{1,0:T(8,128)(2,1)} %all-gather.16.cloned.1.call-done, f32[2048]{0:T(1024)S(1)} %copy-done.14, f32[1024]{0:T(1024)S(1)} %add_rsqrt_fusion), kind=kOutput, calls=%fused_computation.21 | convolution fusion | flops 5918294016 | bytes 15746560 | tf_op jit(solution)/shard_map/dot_general | solution.py:113
  402.4 94.6 %all-gather.22.cloned.1.call-done = bf16[1408,2048]{1,0:T(8,128)(2,1)} async-done(((bf16[1408,512]{1,0:T(8,128)(2,1)}), bf16[1408,2048]{1,0:T(8,128)(2,1)}) %all-gather.22.cloned.1.call-update) | async-done | bytes 5767184 | tf_op jit(solution)/shard_map/all_gather | solution.py:123
  497.0 24.6 %multiply_convert_fusion = bf16[1024,2048]{1,0:T(8,128)(2,1)} fusion(bf16[1408,2048]{1,0:T(8,128)(2,1)} %all-gather.22.cloned.1.call-done, f32[2048]{0:T(1024)S(1)} %bitcast.83, f32[1022,1408]{1,0:T(8,128)} %bitcast.89, f32[1023,1408]{1,0:T(8,128)} %bitcast.90, f32[1024,1408]{1,0:T(8,128)} %fusion.12, f32[1022,1408]{1,0:T(8,128)} %bitcast.87, ...), kind=kOutput, calls=%fused_computation.10 | convolution fusion | flops 5932843008 | bytes 44572672 | tf_op jit(solution)/shard_map/dot_general | solution.py:121
  521.6 42.8 %reduce-scatter.2.cloned.1.call-done = bf16[1024,512]{1,0:T(8,128)(2,1)} async-done(((bf16[1024,2048]{1,0:T(8,128)(2,1)}), bf16[1024,512]{1,0:T(8,128)(2,1)}) %reduce-scatter.2.cloned.1.call-update) | async-done | bytes 1048592 | tf_op jit(solution)/shard_map/reduce_scatter | solution.py:128
  564.4 2.5 fusion.25
  (75 shorter events, 11.3 us)
Async XLA Ops:
  6.5 73.6 %copy-start = (bf16[2,128,128]{2,1,0:T(8,128)(2,1)S(1)}, bf16[2,128,128]{2,1,0:T(8,128)(2,1)}, u32[]{:S(2)}) copy-start(bf16[2,128,128]{2,1,0:T(8,128)(2,1)} %param.21) | copy-start | bytes 196612
  6.5 69.2 %copy-start.15 = (f32[1,256]{1,0:T(1,128)S(1)}, f32[1,256]{1,0:T(1,128)}, u32[]{:S(2)}) copy-start(f32[1,256]{1,0:T(1,128)} %param.20) | copy-start | bytes 3076
  6.5 69.2 %copy-start.13 = (f32[2048]{0:T(1024)S(1)}, f32[2048]{0:T(1024)}, u32[]{:S(2)}) copy-start(f32[2048]{0:T(1024)} %param.18) | copy-start | bytes 24580
  6.5 39.6 %all-gather.24.cloned.1.call-start = ((), (), s32[]{:S(2)}) async-start(), calls=%async_computation.10 | async-start | bytes 5242880 | tf_op jit(solution)/shard_map/all_gather | solution.py:69
  7.3 68.4 %all-gather.10.cloned.1.call-start = ((), (), s32[]{:S(2)}) async-start(), calls=%async_computation.2 | async-start | bytes 1310720 | tf_op jit(solution)/shard_map/all_gather | solution.py:73
  9.1 95.6 %all-gather.14.cloned.1.call-start = ((), (), s32[]{:S(2)}) async-start(), calls=%async_computation.4 | async-start | bytes 1310720 | tf_op jit(solution)/shard_map/all_gather | solution.py:92
  11.1 126.6 %all-gather.12.cloned.1.call-start = ((), (), s32[]{:S(2)}) async-start(), calls=%async_computation.3 | async-start | bytes 2621440 | tf_op jit(solution)/shard_map/all_gather | solution.py:91
  83.4 27.1 %copy-start.10 = (f32[1,512]{1,0:T(1,128)S(1)}, f32[1,512]{1,0:T(1,128)}, u32[]{:S(2)}) copy-start(f32[1,512]{1,0:T(1,128)} %param.24) | copy-start | bytes 6148
  106.9 28.0 %all-to-all-start = ((bf16[256,4,512]{2,0,1:T(8,128)(2,1)}), bf16[256,4,512]{2,0,1:T(8,128)(2,1)S(1)}, u32[]{:S(2)}, u32[]{:S(2)}) async-start(bf16[256,4,512]{2,0,1:T(8,128)(2,1)} %copy.23), calls=%async_computation | async-start | bytes 2097152 | tf_op jit(solution)/shard_map/all_to_all | solution.py:93
  110.5 65.3 %all-gather.16.cloned.1.call-start = ((), (), s32[]{:S(2)}) async-start(), calls=%async_computation.5 | async-start | bytes 5242880 | tf_op jit(solution)/shard_map/all_gather | solution.py:104
  137.6 3.7 copy-start.3
  142.7 141.2 %all-gather.18.cloned.1.call-start = ((), (), s32[]{:S(2)}) async-start(), calls=%async_computation.6 | async-start | bytes 7208960 | tf_op jit(solution)/shard_map/all_gather | solution.py:109
  144.0 3.5 copy-start.5
  144.1 4.8 copy-start.8
  144.1 4.9 copy-start.9
  144.1 4.9 copy-start.11
  144.1 17.0 %copy-start.6 = (f32[3,1408]{1,0:T(4,128)S(1)}, f32[3,1408]{1,0:T(4,128)}, u32[]{:S(2)}) copy-start(f32[3,1408]{1,0:T(4,128)} %param.31) | copy-start | bytes 50692
  144.1 17.0 %copy-start.7 = (f32[3,1408]{1,0:T(4,128)S(1)}, f32[3,1408]{1,0:T(4,128)}, u32[]{:S(2)}) copy-start(f32[3,1408]{1,0:T(4,128)} %param.30) | copy-start | bytes 50692
  144.1 246.3 %all-gather.20.cloned.1.call-start = ((), (), s32[]{:S(2)}) async-start(), calls=%async_computation.7 | async-start | bytes 7208960 | tf_op jit(solution)/shard_map/all_gather | solution.py:110
  147.5 136.4 %copy-start.14 = (f32[2048]{0:T(1024)S(1)}, f32[2048]{0:T(1024)}, u32[]{:S(2)}) copy-start(f32[2048]{0:T(1024)} %param.25) | copy-start | bytes 24580
  147.5 349.5 %all-gather.22.cloned.1.call-start = ((), (), s32[]{:S(2)}) async-start(), calls=%async_computation.8 | async-start | bytes 7208960 | tf_op jit(solution)/shard_map/all_gather | solution.py:123
  148.8 415.6 %reduce-scatter.2.cloned.1.call-start = ((), (), s32[]{:S(2)}) async-start(), calls=%async_computation.9 | async-start | bytes 5242880 | tf_op jit(solution)/shard_map/reduce_scatter | solution.py:128
  497.0 67.4 %copy-start.2 = (bf16[1024,512]{1,0:T(8,128)(2,1)S(1)}, bf16[1024,512]{1,0:T(8,128)(2,1)}, u32[]{:S(2)}) copy-start(bf16[1024,512]{1,0:T(8,128)(2,1)} %fusion.13) | copy-start | bytes 3145732
  497.0 69.9 %copy-start.1 = (bf16[2,128,128]{2,1,0:T(8,128)(2,1)S(1)}, bf16[2,128,128]{2,1,0:T(8,128)(2,1)}, u32[]{:S(2)}) copy-start(bf16[2,128,128]{2,1,0:T(8,128)(2,1)} %param.21) | copy-start | bytes 196612
  (2 other events, 5.4 us)
Sparse Core Ops, SparseCore 0:
  8.9 37.1 all-gather.23
  47.7 27.9 all-gather.9
  77.3 27.3 all-gather.13
  106.1 31.4 all-gather.11
  142.8 32.9 all-gather.15
  177.2 106.6 all-gather.17
  285.5 104.9 all-gather.19
  392.0 104.9 all-gather.21
  521.8 42.6 reduce-scatter.1
where the time goes:
time: 574 us; the launch traced here: 573 us
  waiting for transfers between devices  449 us (78%)
  matrix products  58.5 us (10%)
  blocking collectives  24.1 us (4%)
  other arithmetic  19.3 us (3%)
  between operations  13.5 us (2%)
    all_gather x1, waiting for transfers between devices, shards(): lax.all_gather(gate_cast, 'fs', axis=0, tiled=True)  105 us
    all_gather x1, waiting for transfers between devices, shards(): lax.all_gather(up_cast, 'fs', axis=0, tiled=True)  94.7 us
    all_gather x1, waiting for transfers between devices, shards(): lax.all_gather(down_matrix.astype(jnp.bfloat16), 'fs', axis=1, tiled=True)  94.6 us
    reduce_scatter x1, waiting for transfers between devices, shards(): lax.psum_scatter(partial_ffn.astype(jnp.bfloat16), 'tp', scatter_dimensio...  42.8 us
    all_gather x1, waiting for transfers between devices, shards(): gathered = lax.all_gather(local_rows, 'tp', axis=1, tiled=True)  34.8 us
    all_gather x1, waiting for transfers between devices, shards(): lax.all_gather(in_matrix.astype(jnp.bfloat16), 'fs', axis=0, tiled=True)  26.5 us
    dot_general x1, matrix products, shards(): jnp.dot(hidden, lax.all_gather(down_matrix.astype(jnp.bfloat16), 'fs', ax...  24.6 us
    all_gather x1, waiting for transfers between devices, shards(): lax.all_gather(out_matrix.astype(jnp.bfloat16), 'fs', axis=1, tiled=True)  20.3 us
  transfers between devices with their start and end apart: 10, of which 10 were waited for; matrix products, arithmetic and copies ran while one was open for 9% of the time, Pallas kernels for 0%

commit v1 on v0

v1 whole, which is shorter than its diff:
```python
import jax
import jax.numpy as jnp
from jax import lax
from jax.sharding import PartitionSpec as P


BLOCKS = 8


eps = 1e-06
widest_span = 16


def norm_rows(tok_rows, norm_gain):
    values = tok_rows.astype(jnp.float32)
    scaled = values * lax.rsqrt(jnp.mean(values * values, axis=-1, keepdims=True) + eps)
    return (scaled * norm_gain).astype(jnp.bfloat16)


def span_widths(block_ids):
    return jnp.left_shift(jnp.ones_like(block_ids), 1 + 4 * block_ids // BLOCKS)


def trailing_gap(projected, windows):
    values = projected.astype(jnp.float32)
    length = values.shape[0]
    running = values
    for offset in range(1, widest_span):
        shifted = jnp.pad(values[: length - offset], ((offset, 0), (0, 0)))
        running = running + jnp.where(windows[None, :] > offset, shifted, jnp.zeros_like(shifted))
    positions = jnp.arange(length, dtype=jnp.int32)[:, None]
    counts = jnp.minimum(positions + 1, windows[None, :]).astype(jnp.float32)
    return (running / counts - values).astype(jnp.bfloat16)


def causal_taps(linear, tap_table):
    values = linear.astype(jnp.float32)
    length = values.shape[0]
    back_one = jnp.pad(values[: length - 1], ((1, 0), (0, 0)))
    back_two = jnp.pad(values[: length - 2], ((2, 0), (0, 0)))
    return tap_table[2] * values + tap_table[1] * back_one + tap_table[0] * back_two


def fold_rows(operand, portion):
    return jnp.dot(operand, portion, preferred_element_type=jnp.float32)


def row_halves(shard):
    rows = shard.shape[0] // 2
    mine = lax.axis_index("grp")
    first, second = shard[:rows], shard[rows:]
    return (
        jnp.where(mine == 0, first, second),
        jnp.where(mine == 0, second, first),
    )


def across_groups(value):
    return lax.ppermute(value, "grp", [(0, 1), (1, 0)])


def half_gather(half):
    return lax.all_gather(half, "fs", axis=0, tiled=False)


def others(stacked):
    count = stacked.shape[0]
    here = lax.axis_index("fs")
    return jnp.stack(
        [
            lax.dynamic_index_in_dim(stacked, lax.rem(here + k, count), 0, keepdims=False)
            for k in range(1, count)
        ]
    )


def tp_swap(value, distance):
    count = lax.axis_size("tp")
    return lax.ppermute(value, "tp", [(i, (i + distance) % count) for i in range(count)])


def core_swap(value):
    count = lax.axis_size("tp")
    return lax.ppermute(value, "tp", [(i, i ^ 1) for i in range(count)])


def tp_gather(block, also=None):
    count = lax.axis_size("tp")
    me = lax.axis_index("tp")
    chips = count // 2
    parity = lax.rem(me, 2)
    same = [block] + [tp_swap(block, 2 * j) for j in range(1, chips)]
    if also is not None:
        same, also = tied(same, also)
    crossed = [core_swap(item) for item in same]
    blocks = []
    for chip in range(chips):
        pairs = []
        for group in (same, crossed):
            picked = group[0]
            for j in range(1, chips):
                source = lax.rem(me // 2 - j + chips, chips)
                picked = jnp.where(source == chip, group[j], picked)
            pairs.append(picked)
        blocks.append(jnp.where(parity == 0, pairs[0], pairs[1]))
        blocks.append(jnp.where(parity == 0, pairs[1], pairs[0]))
    return jnp.concatenate(blocks, axis=1), also


def tied(value, other):
    return lax.optimization_barrier((value, other))


def tp_scatter_sum(blocks, also=None):
    count = len(blocks)
    me = lax.axis_index("tp")
    chips = count // 2
    even = lax.rem(me, 2) == 0
    rounded = [item.astype(jnp.bfloat16) for item in blocks]
    pair_sums = []
    for chip in range(chips):
        keep = jnp.where(even, rounded[2 * chip], rounded[2 * chip + 1])
        give = jnp.where(even, rounded[2 * chip + 1], rounded[2 * chip])
        pair_sums.append(keep.astype(jnp.float32) + core_swap(give).astype(jnp.float32))
    chip_index = me // 2

    def for_chip(target):
        picked = pair_sums[0]
        for chip in range(1, chips):
            picked = jnp.where(target == chip, pair_sums[chip], picked)
        return picked

    total = for_chip(chip_index)
    outs = [
        for_chip(lax.rem(chip_index + j, chips)).astype(jnp.bfloat16) for j in range(1, chips)
    ]
    if also is not None:
        outs, also = tied(outs, also)
    for j in range(1, chips):
        total = total + tp_swap(outs[j - 1], 2 * j).astype(jnp.float32)
    return total, also


def shards(
    tokens,
    mix_gain,
    in_matrix,
    in_scale,
    pool_mix,
    pool_scale,
    out_matrix,
    out_scale,
    ffn_gain,
    gate_matrix,
    gate_scale,
    up_matrix,
    up_scale,
    gate_taps,
    up_taps,
    down_matrix,
    down_scale,
):
    half = jnp.bfloat16
    length = tokens.shape[1]
    own_width = tokens.shape[2]
    local_rows = tokens.reshape(length, own_width)
    fs_count = lax.axis_size("fs")
    tp_count = lax.axis_size("tp")
    group = lax.axis_index("grp")
    fs_index = lax.axis_index("fs")

    in_mine, _ = row_halves(in_matrix.astype(half))
    out_mine, _ = row_halves((out_matrix * out_scale).astype(half))
    small_mine = half_gather(jnp.stack([in_mine, out_mine.reshape(in_mine.shape)]))
    small_theirs = across_groups(small_mine)
    small_first = jnp.where(group == 0, small_mine, small_theirs)
    small_second = jnp.where(group == 0, small_theirs, small_mine)
    in_full = jnp.stack([small_first[:, 0], small_second[:, 0]], axis=1).reshape(
        fs_count * in_matrix.shape[0], in_matrix.shape[1]
    )
    out_shape = (fs_count,) + out_mine.shape
    out_full = jnp.concatenate(
        [small_first[:, 1].reshape(out_shape), small_second[:, 1].reshape(out_shape)], axis=1
    )

    wide = []

    def start_wide(cast):
        mine, theirs_here = row_halves(cast)
        mine_all = half_gather(mine)
        wide.append((mine_all, theirs_here))

    start_wide(gate_matrix.astype(half))

    gathered, _ = tp_gather(local_rows)
    gathered, up_cast = tied(gathered, up_matrix.astype(half))
    start_wide(up_cast)
    normed = norm_rows(gathered, mix_gain)
    pieces = 2
    piece_width = down_matrix.shape[1] // pieces
    down_cast = (down_matrix * down_scale).astype(half)
    down_cast, normed = lax.optimization_barrier((down_cast, normed))
    downs = []
    for piece in range(pieces):
        mine, theirs_here = row_halves(
            down_cast[:, piece * piece_width : (piece + 1) * piece_width]
        )
        mine_all = half_gather(mine)
        downs.append((mine_all, theirs_here))

    width_in = in_matrix.shape[1]
    projected = (fold_rows(normed, in_full) * in_scale).astype(half)
    local_blocks = pool_mix.shape[0]
    block_width = pool_mix.shape[1]
    block_ids = lax.axis_index("tp") * local_blocks + jnp.arange(local_blocks, dtype=jnp.int32)
    windows = jnp.repeat(span_widths(block_ids), block_width)
    spread = trailing_gap(projected, windows)
    block_mixed = jnp.einsum(
        "lbc,bce->lbe",
        spread.reshape(length, local_blocks, block_width),
        pool_mix,
        preferred_element_type=jnp.float32,
    ).reshape(length, width_in)
    pooled = (block_mixed * pool_scale).astype(half)
    per_device = fs_count // tp_count
    mixing, gate_send = tp_scatter_sum(
        [
            jnp.concatenate(
                [
                    fold_rows(pooled, out_full[d * per_device + i])
                    for i in range(per_device)
                ],
                axis=1,
            )
            for d in range(tp_count)
        ],
        others(wide[0][0]),
    )
    gate_theirs = across_groups(gate_send)
    residual = (local_rows.astype(jnp.float32) + mixing).astype(half)

    gathered_ffn, up_mine = tp_gather(residual, wide[1][0])
    up_theirs = across_groups(others(up_mine))
    normed_ffn = norm_rows(gathered_ffn, ffn_gain)
    rows = gate_matrix.shape[0] // 2
    split = normed_ffn.reshape(length, fs_count, 2, rows)
    first, second = split[:, :, 0], split[:, :, 1]
    x_mine = jnp.where(group == 0, first, second).reshape(length, fs_count * rows)
    x_theirs = jnp.where(group == 0, second, first)
    x_here = lax.dynamic_index_in_dim(x_theirs, fs_index, 1, keepdims=False)
    x_others = jnp.concatenate(
        [
            lax.dynamic_index_in_dim(
                x_theirs, lax.rem(fs_index + k, fs_count), 1, keepdims=False
            )
            for k in range(1, fs_count)
        ],
        axis=1,
    )
    x_mine, x_here, x_others = lax.optimization_barrier((x_mine, x_here, x_others))
    units = gate_matrix.shape[1]

    def widen(x_parts, parts, scale):
        total = sum(fold_rows(x, w.reshape(-1, units)) for x, w in zip(x_parts, parts))
        return (total * scale).astype(half)

    x_parts = (x_mine, x_here, x_others)
    gate_lin = widen(x_parts, (wide[0][0], wide[0][1], gate_theirs), gate_scale)
    gate_lin, mine_first, x_parts = lax.optimization_barrier((gate_lin, downs[0][0], x_parts))
    theirs_first = across_groups(others(mine_first))
    up_lin = widen(x_parts, (up_mine, wide[1][1], up_theirs), up_scale)
    up_lin, mine_second = tied(up_lin, downs[1][0])
    theirs_second = across_groups(others(mine_second))
    lins = [gate_lin, up_lin]
    hidden = (
        jax.nn.silu(causal_taps(lins[0], gate_taps)) * causal_taps(lins[1], up_taps)
    ).astype(half)
    middle = units // 2
    h_first, h_second = hidden[:, :middle], hidden[:, middle:]
    h_mine = jnp.where(group == 0, h_first, h_second)
    h_theirs = jnp.where(group == 0, h_second, h_first)
    h_mine, h_theirs = lax.optimization_barrier((h_mine, h_theirs))
    results = []
    arrivals = ((mine_first, theirs_first), (mine_second, theirs_second))
    for (_, theirs_here), (mine_all, arrived) in zip(downs, arrivals):
        theirs = jnp.concatenate([theirs_here[None], arrived])
        blocks = []
        for f in range(fs_count):
            slot = lax.rem(f - fs_index + fs_count, fs_count)
            blocks.append(
                fold_rows(h_mine, mine_all[f])
                + fold_rows(
                    h_theirs, lax.dynamic_index_in_dim(theirs, slot, 0, keepdims=False)
                )
            )
        results.append(
            tp_scatter_sum(
                [
                    jnp.concatenate(blocks[d * per_device : (d + 1) * per_device], axis=1)
                    for d in range(tp_count)
                ],
            )[0]
        )
    feed_out = jnp.stack(
        [item.reshape(length, per_device, piece_width) for item in results], axis=2
    ).reshape(length, own_width)
    result = (residual.astype(jnp.float32) + feed_out).astype(half)
    return result.reshape(1, length, result.shape[1])


def solution(mesh):
    return jax.shard_map(
        shards,
        mesh=mesh,
        in_specs=(
            P(("grp", "fs"), None, "tp"),
            P(),
            P("fs", "tp"),
            P(None, "tp"),
            P("tp", None, None),
            P(None, "tp"),
            P("tp", "fs"),
            P(None, "fs"),
            P(),
            P("fs", "tp"),
            P(None, "tp"),
            P("fs", "tp"),
            P(None, "tp"),
            P(None, "tp"),
            P(None, "tp"),
            P("tp", "fs"),
            P(None, "fs"),
        ),
        out_specs=P(("grp", "fs"), None, "tp"),
        check_vma=False,
    )
```

time: 574 us -> 365 us (0.64)
  waiting for transfers between devices: 449 us -> 173 us
  local copies, waits for them, and re-layouts: 4.94 us -> 50 us
  other arithmetic: 19.3 us -> 59.6 us
  blocking collectives: 24.1 us -> 0 us
  starting transfers between devices: 3.85 us -> 17.6 us
  matrix products: 58.5 us -> 46.8 us
    all_gather x8 -> x5, waiting for transfers between devices: 393 us -> 29.4 us  [half_gather(): return lax.all_gather(half, 'fs', axis=0, tiled=False)]
    ppermute x0 -> x20, waiting for transfers between devices: none -> 143 us  [the longest x5 80 us: across_groups(): return lax.ppermute(value, 'grp', [(0, 1), (1, 0)])]
    dot_general x4 -> x0, matrix products: 51.5 us -> none  [the longest x1 24.6 us: shards(): jnp.dot(hidden, lax.all_gather(down_matrix.astype(jnp.bfloat16), 'fs', ax...]
    reduce_scatter x1 -> x0, waiting for transfers between devices: 42.8 us -> none  [shards(): lax.psum_scatter(partial_ffn.astype(jnp.bfloat16), 'tp', scatter_dimensio...]
    dot_general x1 -> x27, matrix products: 3.8 us -> 40.5 us  [fold_rows(): return jnp.dot(operand, portion, preferred_element_type=jnp.float32)]
    all_gather x2 -> x0, blocking collectives: 24.1 us -> none  [the longest x1 12.1 us: shards(): down_cols = lax.all_gather(down_scale, 'fs', axis=1, tiled=True)]
    convert_element_type x6 -> x12, other arithmetic: 9.91 us -> 32.1 us  [the longest x1 9.43 us: shards(): hidden = (jax.nn.silu(causal_taps(lins[0], gate_taps)) * causal_taps(lins...]
    ppermute x0 -> x20, starting transfers between devices: none -> 17.2 us  [the longest x5 8.47 us: tp_swap(): lax.ppermute(value, 'tp', [(i, (i + distance) % count) for i in range(cou...]
  transfers between devices with their start and end apart: 10 -> 25, of which waited for: 10 -> 12; matrix products, arithmetic and copies ran while one was open for 9% -> 38% of each run, Pallas kernels for 0% -> 0%
where the time goes in v1:
time: 365 us; the launch traced here: 361 us
  waiting for transfers between devices  173 us (47%)
  other arithmetic  59.6 us (16%)
  local copies, waits for them, and re-layouts  50 us (14%)
  matrix products  46.8 us (13%)
  starting transfers between devices  17.6 us (5%)
  between operations  14.2 us (4%)
    ppermute x5, waiting for transfers between devices, across_groups(): return lax.ppermute(value, 'grp', [(0, 1), (1, 0)])  80 us
    ppermute x5, waiting for transfers between devices, tp_swap(): lax.ppermute(value, 'tp', [(i, (i + distance) % count) for i in range(cou...  60.5 us
    dot_general x27, matrix products, fold_rows(): return jnp.dot(operand, portion, preferred_element_type=jnp.float32)  40.5 us
    all_gather x5, waiting for transfers between devices, half_gather(): return lax.all_gather(half, 'fs', axis=0, tiled=False)  29.4 us
    unnamed x91, local copies, waits for them, and re-layouts  9.78 us
    convert_element_type x1, other arithmetic, shards(): hidden = (jax.nn.silu(causal_taps(lins[0], gate_taps)) * causal_taps(lins...  9.43 us
    ppermute x5, starting transfers between devices, tp_swap(): lax.ppermute(value, 'tp', [(i, (i + distance) % count) for i in range(cou...  8.47 us
    slice x8, local copies, waits for them, and re-layouts, trailing_gap(): shifted = jnp.pad(values[:length - offset], ((offset, 0), (0, 0)))  8.44 us
  transfers between devices with their start and end apart: 25, of which 12 were waited for; matrix products, arithmetic and copies ran while one was open for 38% of the time, Pallas kernels for 0%

profile of v1, /device:TPU:0, one launch (start us, length us, event | category | flops | bytes accessed | tf_op | source)
XLA Modules:
  0.0 360.8 jit_solution(4559457760173157797)
XLA Ops:
  9.7 3.0 collective-permute-start
  19.0 17.1 %collective-permute-done = bf16[1024,512]{1,0:T(8,128)(2,1)} collective-permute-done((bf16[1024,512]{1,0:T(8,128)(2,1)S(1)}, bf16[1024,512]{1,0:T(8,128)(2,1)}, u32[]{:S(2)}, u32[]{:S(2)}) %collective-permute-start) | collective-permute-done | bytes 1048608 | tf_op jit(solution)/shard_map/ppermute | solution.py:79
  36.2 3.4 multiply_convert_fusion.4
  45.7 3.0 fusion.2
  49.9 15.6 %collective-permute-done.3 = bf16[4,2,256,256]{3,2,1,0:T(8,128)(2,1)} collective-permute-done((bf16[4,2,256,256]{3,2,1,0:T(8,128)(2,1)}, bf16[4,2,256,256]{3,2,1,0:T(8,128)(2,1)}, u32[]{:S(2)}, u32[]{:S(2)}) %collective-permute-start.3) | collective-permute-done | bytes 1048608 | tf_op jit(solution)/shard_map/ppermute | solution.py:59
  79.5 6.4 %fusion.13 = bf16[2,1024,128]{1,2,0:T(8,128)(2,1)S(1)} fusion(bf16[2,128,128]{2,1,0:T(8,128)(2,1)S(1)} %copy-done, f32[2,128]{1,0:T(2,128)S(1)} %bitcast.231, f32[1024,256]{1,0:T(8,128)S(1)} %fusion.4, s32[256]{0:T(256)S(1)} %broadcast_bitcast_fusion, s32[1024]{0:T(1024)S(1)} %iota_add_fusion, f32[1009,256]{1,0:T(8,128)} %slice.254, ...), kind=kOutput, calls=%fused_computation.65 | convolution fusion | flops 76808192 | bytes 17254144 | tf_op jit(solution)/shard_map/lbc,bce->lbe/dot_general | solution.py:218
  95.2 3.3 select_convert_fusion
  106.7 22.1 %collective-permute-done.6 = bf16[1024,512]{1,0:T(8,128)(2,1)} collective-permute-done((bf16[1024,512]{1,0:T(8,128)(2,1)S(1)}, bf16[1024,512]{1,0:T(8,128)(2,1)}, u32[]{:S(2)}, u32[]{:S(2)}) %collective-permute-start.6) | collective-permute-done | bytes 1048608 | tf_op jit(solution)/shard_map/ppermute | solution.py:79
  128.8 3.3 add_convert_fusion.1
  133.6 26.4 %all-gather.15.cloned.1.call-done = bf16[1024,1408]{1,0:T(8,128)(2,1)} async-done(((bf16[256,1408]{1,0:T(8,128)(2,1)}), bf16[1024,1408]{1,0:T(8,128)(2,1)}) %all-gather.15.cloned.1.call-update) | async-done | bytes 2883600 | tf_op jit(solution)/shard_map/all_gather | solution.py:63
  167.3 2.9 broadcast_select_fusion.17
  175.3 3.2 multiply_reduce_fusion
  192.2 3.5 fusion.95
  195.7 15.4 %collective-permute-done.10 = bf16[3,256,1408]{2,1,0:T(8,128)(2,1)} collective-permute-done((bf16[3,256,1408]{2,1,0:T(8,128)(2,1)}, bf16[3,256,1408]{2,1,0:T(8,128)(2,1)}, u32[]{:S(2)}, u32[]{:S(2)}) %collective-permute-start.10) | collective-permute-done | bytes 2162720 | tf_op jit(solution)/shard_map/ppermute | solution.py:59
  211.1 4.9 %multiply_convert_fusion.3 = bf16[1024,1408]{1,0:T(8,128)(2,1)S(1)} fusion(f32[1024,1408]{1,0:T(8,128)S(1)} %fusion.95, f32[1024,1408]{1,0:T(8,128)S(1)} %fusion.17, bf16[1024,768]{1,0:T(8,128)(2,1)S(1)} %pad_maximum_fusion.4, bf16[768,1408]{1,0:T(8,128)(2,1)} %bitcast.27, f32[1408]{0:T(1024)S(1)} %reduce.1), kind=kOutput, calls=%fused_computation.9 | convolution fusion | flops 2220359680 | bytes 18159104 | tf_op jit(solution)/shard_map/dot_general | solution.py:45
  226.6 3.5 fusion.96
  230.2 27.2 %collective-permute-done.11 = bf16[3,256,1408]{2,1,0:T(8,128)(2,1)} collective-permute-done((bf16[3,256,1408]{2,1,0:T(8,128)(2,1)}, bf16[3,256,1408]{2,1,0:T(8,128)(2,1)}, u32[]{:S(2)}, u32[]{:S(2)}) %collective-permute-start.11) | collective-permute-done | bytes 2162720 | tf_op jit(solution)/shard_map/ppermute | solution.py:59
  257.4 5.6 %multiply_convert_fusion.2 = bf16[1024,1408]{1,0:T(8,128)(2,1)} fusion(f32[1024,1408]{1,0:T(8,128)S(1)} %fusion.96, f32[1024,1408]{1,0:T(8,128)S(1)} %fusion.15, bf16[1024,768]{1,0:T(8,128)(2,1)S(1)} %copy-done.26, bf16[768,1408]{1,0:T(8,128)(2,1)} %bitcast.30, f32[1408]{0:T(1024)S(1)} %reduce.5), kind=kOutput, calls=%fused_computation.8 | convolution fusion | flops 2220359680 | bytes 18159104 | tf_op jit(solution)/shard_map/dot_general | solution.py:45
  263.1 5.3 %slice.267 = f32[1023,1408]{1,0:T(8,128)} slice(bf16[1024,1408]{1,0:T(8,128)(2,1)} %multiply_convert_fusion.2), slice={[0:1023], [0:1408]} | slice | bytes 11523072 | tf_op jit(solution)/shard_map/slice | solution.py:39
  268.3 3.3 slice.268
  273.3 9.4 %multiply_convert_fusion.1 = bf16[1024,1408]{1,0:T(8,128)(2,1)S(1)} fusion(f32[1022,1408]{1,0:T(8,128)} %slice.268, f32[1023,1408]{1,0:T(8,128)} %slice.267, f32[1022,1408]{1,0:T(8,128)S(1)} %bitcast.194, f32[1023,1408]{1,0:T(8,128)S(1)} %bitcast.192, f32[1408]{0:T(1024)S(1)} %get-tuple-element.51, f32[1408]{0:T(1024)S(1)} %get-tuple-element.52, ...), kind=kLoop, calls=%fused_computation.7 | loop fusion | flops 25952256 | bytes 31719424 | tf_op jit(solution)/shard_map/convert_element_type | solution.py:277
  297.6 21.8 %collective-permute-done.16 = bf16[3,704,256]{2,1,0:T(8,128)(2,1)S(1)} collective-permute-done((bf16[3,704,256]{2,1,0:T(8,128)(2,1)S(1)}, bf16[3,704,256]{2,1,0:T(8,128)(2,1)S(1)}, u32[]{:S(2)}, u32[]{:S(2)}) %collective-permute-start.16) | collective-permute-done | bytes 1081376 | tf_op jit(solution)/shard_map/ppermute | solution.py:59
  326.4 11.8 %collective-permute-done.15 = bf16[1024,256]{0,1:T(8,128)(2,1)S(1)} collective-permute-done((bf16[1024,256]{0,1:T(8,128)(2,1)S(1)}, bf16[1024,256]{0,1:T(8,128)(2,1)S(1)}, u32[]{:S(2)}, u32[]{:S(2)}) %collective-permute-start.15) | collective-permute-done | bytes 524320 | tf_op jit(solution)/shard_map/ppermute | solution.py:79
  338.9 9.6 %collective-permute-done.19 = bf16[1024,256]{0,1:T(8,128)(2,1)S(1)} collective-permute-done((bf16[1024,256]{0,1:T(8,128)(2,1)S(1)}, bf16[1024,256]{0,1:T(8,128)(2,1)S(1)}, u32[]{:S(2)}, u32[]{:S(2)}) %collective-permute-start.19) | collective-permute-done | bytes 524320 | tf_op jit(solution)/shard_map/ppermute | solution.py:79
  (230 shorter events, 115.6 us)
Async XLA Ops:
  6.5 34.0 %all-gather.11.cloned.1.call-start = ((), (), s32[]{:S(2)}) async-start(), calls=%async_computation | async-start | bytes 1310720 | tf_op jit(solution)/shard_map/all_gather | solution.py:63
  9.7 91.0 %all-gather.13.cloned.1.call-start = ((), (), s32[]{:S(2)}) async-start(), calls=%async_computation.1 | async-start | bytes 3604480 | tf_op jit(solution)/shard_map/all_gather | solution.py:63
  9.7 26.3 %collective-permute-start = (bf16[1024,512]{1,0:T(8,128)(2,1)S(1)}, bf16[1024,512]{1,0:T(8,128)(2,1)}, u32[]{:S(2)}, u32[]{:S(2)}) collective-permute-start(bf16[1024,512]{1,0:T(8,128)(2,1)S(1)} %bitcast.212), channel_id=1, source_target_pairs={{0,2},{1,3},{2,0},{3,1},{4,6},{5,7},{6,4},{7,5},{8,10},{9,11},{10,... | collective-permute-start | bytes 3145736 | tf_op jit(solution)/shard_map/ppermute | solution.py:79
  16.8 143.2 %all-gather.15.cloned.1.call-start = ((), (), s32[]{:S(2)}) async-start(), calls=%async_computation.2 | async-start | bytes 3604480 | tf_op jit(solution)/shard_map/all_gather | solution.py:63
  16.8 25.2 %collective-permute-start.2 = (bf16[1024,512]{1,0:T(8,128)(2,1)S(1)}, bf16[1024,512]{1,0:T(8,128)(2,1)}, u32[]{:S(2)}, u32[]{:S(2)}) collective-permute-start(bf16[1024,512]{1,0:T(8,128)(2,1)S(1)} %bitcast.213), channel_id=1, source_target_pairs={{0,1},{1,0},{2,3},{3,2},{4,5},{5,4},{6,7},{7,6},{8,9},{9,8},{10,11... | collective-permute-start | bytes 3145736 | tf_op jit(solution)/shard_map/ppermute | solution.py:84
  36.0 6.0 %collective-permute-start.1 = (bf16[1024,512]{1,0:T(8,128)(2,1)}, bf16[1024,512]{1,0:T(8,128)(2,1)}, u32[]{:S(2)}, u32[]{:S(2)}) collective-permute-start(bf16[1024,512]{1,0:T(8,128)(2,1)} %collective-permute-done), channel_id=1, source_target_pairs={{0,1},{1,0},{2,3},{3,2},{4,5},{5,4},{6,7},{7,6},{8,9},{9,8},{10,11... | collective-permute-start | bytes 3145736 | tf_op jit(solution)/shard_map/ppermute | solution.py:84
  40.5 25.0 %collective-permute-start.3 = (bf16[4,2,256,256]{3,2,1,0:T(8,128)(2,1)}, bf16[4,2,256,256]{3,2,1,0:T(8,128)(2,1)}, u32[]{:S(2)}, u32[]{:S(2)}) collective-permute-start(bf16[4,2,256,256]{3,2,1,0:T(8,128)(2,1)} %bitcast.225), channel_id=1, source_target_pairs={{0,16},{16,0},{1,17},{17,1},{2,18},{18,2},{3,19},{19,3},{4,20},{20... | collective-permute-start | bytes 3145736 | tf_op jit(solution)/shard_map/ppermute | solution.py:59
  49.7 166.4 %all-gather.17.cloned.1.call-start = ((), (), s32[]{:S(2)}) async-start(), calls=%async_computation.3 | async-start | bytes 1802240 | tf_op jit(solution)/shard_map/all_gather | solution.py:63
  87.9 4.7 %collective-permute-start.5 = (bf16[1024,512]{1,0:T(8,128)(2,1)}, bf16[1024,512]{1,0:T(8,128)(2,1)}, u32[]{:S(2)}, u32[]{:S(2)}) collective-permute-start(bf16[1024,512]{1,0:T(8,128)(2,1)} %get-tuple-element.108), channel_id=1, source_target_pairs={{0,1},{1,0},{2,3},{3,2},{4,5},{5,4},{6,7},{7,6},{8,9},{9,8},{10,11... | collective-permute-start | bytes 3145736 | tf_op jit(solution)/shard_map/ppermute | solution.py:84
  92.2 3.0 collective-permute-start.4
  104.0 24.8 %collective-permute-start.6 = (bf16[1024,512]{1,0:T(8,128)(2,1)S(1)}, bf16[1024,512]{1,0:T(8,128)(2,1)}, u32[]{:S(2)}, u32[]{:S(2)}) collective-permute-start(bf16[1024,512]{1,0:T(8,128)(2,1)S(1)} %copy-done.31), channel_id=1, source_target_pairs={{0,2},{1,3},{2,0},{3,1},{4,6},{5,7},{6,4},{7,5},{8,10},{9,11},{10,... | collective-permute-start | bytes 3145736 | tf_op jit(solution)/shard_map/ppermute | solution.py:79
  106.6 156.4 %all-gather.19.cloned.1.call-start = ((), (), s32[]{:S(2)}) async-start(), calls=%async_computation.4 | async-start | bytes 1802240 | tf_op jit(solution)/shard_map/all_gather | solution.py:63
  132.1 27.9 %collective-permute-start.7 = (bf16[1024,512]{1,0:T(8,128)(2,1)S(1)}, bf16[1024,512]{1,0:T(8,128)(2,1)S(1)}, u32[]{:S(2)}, u32[]{:S(2)}) collective-permute-start(bf16[1024,512]{1,0:T(8,128)(2,1)S(1)} %add_convert_fusion.1), channel_id=1, source_target_pairs={{0,2},{1,3},{2,0},{3,1},{4,6},{5,7},{6,4},{7,5},{8,10},{9,11},{10,... | collective-permute-start | bytes 3145736 | tf_op jit(solution)/shard_map/ppermute | solution.py:79
  160.0 6.3 %collective-permute-start.8 = (bf16[1024,512]{1,0:T(8,128)(2,1)S(1)}, bf16[1024,512]{1,0:T(8,128)(2,1)S(1)}, u32[]{:S(2)}, u32[]{:S(2)}) collective-permute-start(bf16[1024,512]{1,0:T(8,128)(2,1)S(1)} %collective-permute-done.7), channel_id=1, source_target_pairs={{0,1},{1,0},{2,3},{3,2},{4,5},{5,4},{6,7},{7,6},{8,9},{9,8},{10,11... | collective-permute-start | bytes 3145736 | tf_op jit(solution)/shard_map/ppermute | solution.py:84
  160.0 7.2 %collective-permute-start.9 = (bf16[1024,512]{1,0:T(8,128)(2,1)S(1)}, bf16[1024,512]{1,0:T(8,128)(2,1)}, u32[]{:S(2)}, u32[]{:S(2)}) collective-permute-start(bf16[1024,512]{1,0:T(8,128)(2,1)S(1)} %add_convert_fusion.1), channel_id=1, source_target_pairs={{0,1},{1,0},{2,3},{3,2},{4,5},{5,4},{6,7},{7,6},{8,9},{9,8},{10,11... | collective-permute-start | bytes 3145736 | tf_op jit(solution)/shard_map/ppermute | solution.py:84
  160.8 50.3 %collective-permute-start.10 = (bf16[3,256,1408]{2,1,0:T(8,128)(2,1)}, bf16[3,256,1408]{2,1,0:T(8,128)(2,1)}, u32[]{:S(2)}, u32[]{:S(2)}) collective-permute-start(bf16[3,256,1408]{2,1,0:T(8,128)(2,1)} %pad_maximum_fusion.1), channel_id=1, source_target_pairs={{0,16},{16,0},{1,17},{17,1},{2,18},{18,2},{3,19},{19,3},{4,20},{20... | collective-permute-start | bytes 6488072 | tf_op jit(solution)/shard_map/ppermute | solution.py:59
  165.7 91.7 %collective-permute-start.11 = (bf16[3,256,1408]{2,1,0:T(8,128)(2,1)}, bf16[3,256,1408]{2,1,0:T(8,128)(2,1)}, u32[]{:S(2)}, u32[]{:S(2)}) collective-permute-start(bf16[3,256,1408]{2,1,0:T(8,128)(2,1)} %pad_maximum_fusion.2), channel_id=1, source_target_pairs={{0,16},{16,0},{1,17},{17,1},{2,18},{18,2},{3,19},{19,3},{4,20},{20... | collective-permute-start | bytes 6488072 | tf_op jit(solution)/shard_map/ppermute | solution.py:59
  224.1 62.5 %collective-permute-start.12 = (bf16[3,704,256]{2,1,0:T(8,128)(2,1)}, bf16[3,704,256]{2,1,0:T(8,128)(2,1)}, u32[]{:S(2)}, u32[]{:S(2)}) collective-permute-start(bf16[3,704,256]{2,1,0:T(8,128)(2,1)} %pad_maximum_fusion.5), channel_id=1, source_target_pairs={{0,16},{16,0},{1,17},{17,1},{2,18},{18,2},{3,19},{19,3},{4,20},{20... | collective-permute-start | bytes 3244040 | tf_op jit(solution)/shard_map/ppermute | solution.py:59
  289.3 33.5 %collective-permute-start.14 = (bf16[1024,256]{0,1:T(8,128)(2,1)S(1)}, bf16[1024,256]{0,1:T(8,128)(2,1)S(1)}, u32[]{:S(2)}, u32[]{:S(2)}) collective-permute-start(bf16[1024,256]{0,1:T(8,128)(2,1)S(1)} %get-tuple-element.116), channel_id=1, source_target_pairs={{0,1},{1,0},{2,3},{3,2},{4,5},{5,4},{6,7},{7,6},{8,9},{9,8},{10,11... | collective-permute-start | bytes 1572872 | tf_op jit(solution)/shard_map/ppermute | solution.py:84
  292.8 29.9 %collective-permute-start.13 = (bf16[1024,256]{0,1:T(8,128)(2,1)S(1)}, bf16[1024,256]{0,1:T(8,128)(2,1)S(1)}, u32[]{:S(2)}, u32[]{:S(2)}) collective-permute-start(bf16[1024,256]{0,1:T(8,128)(2,1)S(1)} %get-tuple-element.114), channel_id=1, source_target_pairs={{0,1},{1,0},{2,3},{3,2},{4,5},{5,4},{6,7},{7,6},{8,9},{9,8},{10,11... | collective-permute-start | bytes 1572872 | tf_op jit(solution)/shard_map/ppermute | solution.py:84
  293.5 25.9 %collective-permute-start.16 = (bf16[3,704,256]{2,1,0:T(8,128)(2,1)S(1)}, bf16[3,704,256]{2,1,0:T(8,128)(2,1)S(1)}, u32[]{:S(2)}, u32[]{:S(2)}) collective-permute-start(bf16[3,704,256]{2,1,0:T(8,128)(2,1)S(1)} %pad_maximum_fusion.6), channel_id=1, source_target_pairs={{0,16},{16,0},{1,17},{17,1},{2,18},{18,2},{3,19},{19,3},{4,20},{20... | collective-permute-start | bytes 3244040 | tf_op jit(solution)/shard_map/ppermute | solution.py:59
  320.7 4.1 %collective-permute-start.18 = (bf16[1024,256]{0,1:T(8,128)(2,1)S(1)}, bf16[1024,256]{0,1:T(8,128)(2,1)S(1)}, u32[]{:S(2)}, u32[]{:S(2)}) collective-permute-start(bf16[1024,256]{0,1:T(8,128)(2,1)S(1)} %get-tuple-element.112), channel_id=1, source_target_pairs={{0,1},{1,0},{2,3},{3,2},{4,5},{5,4},{6,7},{7,6},{8,9},{9,8},{10,11... | collective-permute-start | bytes 1572872 | tf_op jit(solution)/shard_map/ppermute | solution.py:84
  323.3 14.9 %collective-permute-start.15 = (bf16[1024,256]{0,1:T(8,128)(2,1)S(1)}, bf16[1024,256]{0,1:T(8,128)(2,1)S(1)}, u32[]{:S(2)}, u32[]{:S(2)}) collective-permute-start(bf16[1024,256]{0,1:T(8,128)(2,1)S(1)} %select_convert_fusion.2), channel_id=1, source_target_pairs={{0,2},{1,3},{2,0},{3,1},{4,6},{5,7},{6,4},{7,5},{8,10},{9,11},{10,... | collective-permute-start | bytes 1572872 | tf_op jit(solution)/shard_map/ppermute | solution.py:79
  325.5 23.0 %collective-permute-start.19 = (bf16[1024,256]{0,1:T(8,128)(2,1)S(1)}, bf16[1024,256]{0,1:T(8,128)(2,1)S(1)}, u32[]{:S(2)}, u32[]{:S(2)}) collective-permute-start(bf16[1024,256]{0,1:T(8,128)(2,1)S(1)} %select_convert_fusion.1), channel_id=1, source_target_pairs={{0,2},{1,3},{2,0},{3,1},{4,6},{5,7},{6,4},{7,5},{8,10},{9,11},{10,... | collective-permute-start | bytes 1572872 | tf_op jit(solution)/shard_map/ppermute | solution.py:79
  (46 other events, 616.9 us)
Sparse Core Ops, SparseCore 0:
  9.8 30.6 all-gather.10
  42.1 58.4 all-gather.12
  102.2 57.7 all-gather.14
  161.4 33.4 all-gather.16
  196.3 33.7 all-gather.18
